TPU v7x, 32 devices: a whole 2x2x4 slice. The times are simulated.
32 devices in a mesh: ep: 8 (over z, y), tp: 4 (over x, core).
Axes of the slice: x: 2, y: 2, z: 4, core: 2. Of those that a mesh axis runs over, the one named last changes fastest.
Arguments:
- c_gate: bfloat16 [2048, 1024], P('ep', 'tp'), may hold values from -6 to 6
- b_gate: bfloat16 [2048, 1024], P('ep', 'tp'), may hold values from -6 to 6
- values: bfloat16 [2048, 1024], P('ep', 'tp'), may hold values from -6 to 6
- conv_taps: float32 [3, 1024], P(None, 'tp'), may hold values from -3.5 to 3.5
- w_mix_out: bfloat16 [1024, 2048], P('tp'), may hold values from -0.1875 to 0.1875
- moe_in: bfloat16 [4096, 2048], P(('ep', 'tp')), may hold values from -6 to 6
- norm_gain: float32 [2048], replicated, may hold values from 0.1 to 1.9
- route_ids: int32 [4096, 2], P(('ep', 'tp')), may hold values from 0 to 7, all different within a row; in each aligned block of 128 rows (0 to 127, 128 to 255, ...) at most 40 rows name the same one
- route_weights: float32 [4096, 2], P(('ep', 'tp')), may hold values from 0.1 to 1
- w_gate: bfloat16 [8, 2048, 3584], P('ep', None, 'tp'), may hold values from -0.125 to 0.125
- w_up: bfloat16 [8, 2048, 3584], P('ep', None, 'tp'), may hold values from -0.125 to 0.125
- w_down: bfloat16 [8, 3584, 2048], P('ep', 'tp'), may hold values from -0.09375 to 0.09375
Outputs:
- mixer_out: bfloat16 [2048, 2048], P(('ep', 'tp'))
- moe_out: bfloat16 [4096, 2048], P(('ep', 'tp'))
Inputs may be any that keep to these rules, and one draw needn't show every extreme that they name: `route_ids`: each row names 2 different experts; in each aligned block of 128 rows (the rows of one device) no expert is named by more than 40 rows, and in every draw some expert is named by exactly 40 rows in some block.
All inputs are finite; a program needn't handle non-finite values.
Results may differ from a plain program's by a relative error of at most 0.012.
Values may be sent and summed in bfloat16 or wider, within the bound.
A program may use at most 128 MiB of HBM per device.

v0:
```python
import jax
import jax.numpy as jnp
from jax import lax
from jax.sharding import PartitionSpec as P

EPS = 1e-06


def passed_along(block, axis, distance):
    devices = range(lax.axis_size(axis))
    route = [(i - distance, i) for i in devices if i - distance in devices]
    return lax.ppermute(block, axis, route)


def rank_copies(route_block, experts):
    flat_ids = route_block.reshape(-1)
    onehot = (flat_ids[:, None] == jnp.arange(experts, dtype=jnp.int32)[None, :]).astype(jnp.int32)
    before = jnp.cumsum(onehot, axis=0) - onehot
    return (flat_ids, jnp.sum(before * onehot, axis=1))


def pack_rows(rows, slot_of, top, slot_count):
    copies = slot_of.shape[0]
    table = (
        jnp.full((slot_count,), copies, jnp.int32)
        .at[slot_of]
        .set(jnp.arange(copies, dtype=jnp.int32))
    )
    padded = jnp.concatenate([rows, jnp.zeros((1, rows.shape[1]), rows.dtype)], 0)
    return padded[table // top]


def on_device(
    c_gate,
    b_gate,
    values,
    conv_taps,
    w_mix_out,
    moe_in,
    norm_gain,
    route_ids,
    route_weights,
    w_gate,
    w_up,
    w_down,
):
    tokens = c_gate.shape[0]
    reach = conv_taps.shape[0] - 1
    product = c_gate.astype(jnp.float32) * values.astype(jnp.float32)
    previous = passed_along(product[tokens - reach :], "ep", 1)
    extended = jnp.concatenate([previous, product], 0)
    convolved = jnp.zeros_like(product)
    for offset in range(reach + 1):
        convolved = convolved + conv_taps[offset][None, :] * extended[offset : offset + tokens]
    mixed = (b_gate.astype(jnp.float32) * convolved).astype(jnp.bfloat16)
    piece = mixed
    mixer_out = lax.psum_scatter(
        jnp.dot(piece, w_mix_out, preferred_element_type=jnp.float32).astype(jnp.bfloat16),
        "tp",
        scatter_dimension=0,
        tiled=True,
    )
    rows_b = moe_in.shape[0]
    width = moe_in.shape[1]
    top = route_ids.shape[1]
    n_ep = lax.axis_size("ep")
    experts = w_gate.shape[0] * n_ep
    capacity = 5 * rows_b * top // (4 * experts)
    stream = moe_in.astype(jnp.float32)
    scale = lax.rsqrt(jnp.mean(stream * stream, axis=1, keepdims=True) + EPS)
    normed = (stream * scale * norm_gain[None, :]).astype(jnp.bfloat16)
    own_ids, own_ranks = rank_copies(route_ids, experts)
    own_slot = own_ids * capacity + own_ranks
    outgoing = pack_rows(normed, own_slot, top, experts * capacity).reshape(
        experts, capacity, width
    )
    arrived = lax.all_to_all(outgoing, "ep", split_axis=0, concat_axis=1, tiled=True).reshape(
        -1, width
    )
    piece = lax.all_gather(arrived, "tp", axis=0, tiled=True)
    gate_val = jnp.dot(piece, w_gate[0], preferred_element_type=jnp.float32)
    up_val = jnp.dot(piece, w_up[0], preferred_element_type=jnp.float32)
    hidden = (jax.nn.silu(gate_val) * up_val).astype(jnp.bfloat16)
    piece = hidden
    expert_out = lax.psum_scatter(
        jnp.dot(piece, w_down[0], preferred_element_type=jnp.float32).astype(jnp.bfloat16),
        "tp",
        scatter_dimension=0,
        tiled=True,
    )
    returned = lax.all_to_all(
        expert_out.reshape(n_ep, capacity, width), "ep", split_axis=0, concat_axis=0, tiled=True
    )
    picked = returned.reshape(-1, width)[own_slot].astype(jnp.float32).reshape(rows_b, top, width)
    moe_out = jnp.sum(picked * route_weights[:, :, None], axis=1).astype(jnp.bfloat16)
    return (mixer_out, moe_out)


def solution(mesh):
    return jax.shard_map(
        on_device,
        mesh=mesh,
        in_specs=(
            P("ep", "tp"),
            P("ep", "tp"),
            P("ep", "tp"),
            P(None, "tp"),
            P("tp", None),
            P(("ep", "tp"), None),
            P(),
            P(("ep", "tp"), None),
            P(("ep", "tp"), None),
            P("ep", None, "tp"),
            P("ep", None, "tp"),
            P("ep", "tp", None),
        ),
        out_specs=(P(("ep", "tp"), None), P(("ep", "tp"), None)),
        check_vma=False,
    )
```

profile of v0, /device:TPU:0, one launch (start us, length us, event | category | flops | bytes accessed | tf_op | source)
XLA Modules:
  0.0 225.9 jit_solution(5332753036802523370)
XLA Ops:
  7.2 0.0 copy-start
  7.2 0.0 all-gather.2.cloned.1.call-start
  7.2 0.9 copy.16
  8.1 0.1 eq.29
  8.2 0.1 eq.25
  8.4 0.7 broadcast_multiply_fusion
  9.1 0.6 reduce-window.6
  9.6 0.2 slice_reduce_fusion
  9.9 0.1 copy.15
  10.0 0.1 mul.107
  10.1 0.1 fusion.19
  10.3 1.4 scatter_custom_fusion
  11.7 1.2 fusion.4
  12.9 1.2 fusion.6
  14.2 2.4 %gather_fusion = bf16[320,2048]{1,0:T(8,128)(2,1)S(1)} fusion(bf16[129,2048]{1,0:T(8,128)(2,1)S(1)} %concatenate.7, s32[1024]{0:T(1024)S(1)} %pad_clamp_fusion.1), kind=kCustom, calls=%fused_computation | custom fusion | bytes 2622720 | tf_op jit(solution)/shard_map/gather | solution.py:30
  16.7 38.6 %all_to_all.14 = bf16[8,40,2048]{2,1,0:T(8,128)(2,1)} all-to-all(bf16[8,40,2048]{2,1,0:T(8,128)(2,1)S(1)} %bitcast.39), channel_id=1, replica_groups=mesh['ep'=8,'tp'=4] {'ep'}, dimensions={0} | all-to-all | bytes 2621440 | tf_op jit(solution)/shard_map/all_to_all | solution.py:77
  55.3 0.0 all-gather.2.cloned.1.call-update
  55.3 0.0 reduce-scatter.5.cloned.1.call-start
  55.3 39.5 %all-gather.2.cloned.1.call-done = bf16[1280,2048]{1,0:T(8,128)(2,1)} async-done(((bf16[320,2048]{1,0:T(8,128)(2,1)}), bf16[1280,2048]{1,0:T(8,128)(2,1)}) %all-gather.2.cloned.1.call-update) | async-done | bytes 5242896 | tf_op jit(solution)/shard_map/all_gather | solution.py:80
  94.9 10.0 %fusion.2 = f32[1280,896]{1,0:T(8,128)} fusion(bf16[1280,2048]{1,0:T(8,128)(2,1)} %all-gather.2.cloned.1.call-done, bf16[1,2048,896]{2,1,0:T(8,128)(2,1)} %param.21), kind=kOutput, calls=%fused_computation.7 | convolution fusion | flops 4697620480 | bytes 13500416 | tf_op jit(solution)/shard_map/dot_general | solution.py:81
  104.8 17.6 %convolution_convert_fusion = bf16[1280,2048]{1,0:T(8,128)(2,1)} fusion(bf16[1,896,2048]{2,1,0:T(8,128)(2,1)} %param.23, f32[1280,896]{1,0:T(8,128)} %fusion.2, bf16[1280,2048]{1,0:T(8,128)(2,1)} %all-gather.2.cloned.1.call-done, bf16[1,2048,896]{2,1,0:T(8,128)(2,1)} %param.22), kind=kOutput, calls=%fused_computation.3 | convolution fusion | flops 9404743680 | bytes 22413312 | tf_op jit(solution)/shard_map/dot_general | solution.py:86
  122.4 0.0 copy-start.2
  122.4 0.0 copy-start.3
  122.4 0.0 copy-start.4
  122.4 0.0 copy-start.1
  122.4 0.0 reduce-scatter.5.cloned.1.call-update
  122.4 0.9 copy-done.2
  123.3 0.1 copy-done.3
  123.4 0.0 copy-start.5
  123.4 3.4 %collective-permute-start = (f32[2,256]{1,0:T(2,128)S(1)}, f32[2,256]{1,0:T(2,128)S(1)}, u32[]{:S(2)}, u32[]{:S(2)}) collective-permute-start(f32[2,256]{1,0:T(2,128)S(1)} %slice.36), channel_id=1, source_target_pairs={{0,4},{4,8},{8,12},{12,16},{16,20},{20,24},{24,28},{1,5},{5,9},{9,... | collective-permute-start | bytes 6152 | tf_op jit(solution)/shard_map/ppermute | solution.py:12
  126.8 47.2 %reduce-scatter.5.cloned.1.call-done = bf16[320,2048]{1,0:T(8,128)(2,1)} async-done(((bf16[1280,2048]{1,0:T(8,128)(2,1)}), bf16[320,2048]{1,0:T(8,128)(2,1)}) %reduce-scatter.5.cloned.1.call-update) | async-done | bytes 1310736 | tf_op jit(solution)/shard_map/reduce_scatter | solution.py:85
  174.0 5.5 %all-to-all-start.1 = ((bf16[8,40,2048]{2,1,0:T(8,128)(2,1)}), bf16[8,40,2048]{2,1,0:T(8,128)(2,1)S(1)}, u32[]{:S(2)}, u32[]{:S(2)}) async-start(bf16[8,40,2048]{2,1,0:T(8,128)(2,1)} %bitcast.41), calls=%async_computation.3 | async-start | bytes 2621440 | tf_op jit(solution)/shard_map/all_to_all | solution.py:91
  179.5 0.2 reduce-scatter.3.cloned.1.call-start
  179.7 0.0 copy-done.4
  179.7 0.0 collective-permute-done
  179.7 0.0 copy-done
  179.7 0.0 copy-done.1
  179.8 1.5 convolution_convert_fusion.1
  181.2 0.0 reduce-scatter.3.cloned.1.call-update
  181.2 0.0 copy-done.5
  181.3 0.1 copy.18
  181.4 29.3 %all-to-all-done.1 = bf16[8,40,2048]{2,1,0:T(8,128)(2,1)S(1)} async-done(((bf16[8,40,2048]{2,1,0:T(8,128)(2,1)}), bf16[8,40,2048]{2,1,0:T(8,128)(2,1)S(1)}, u32[]{:S(2)}, u32[]{:S(2)}) %all-to-all-start.1) | async-done | bytes 1310752 | tf_op jit(solution)/shard_map/all_to_all | solution.py:91
  210.7 2.3 %gather_fusion.1 = bf16[256,2048]{1,0:T(8,128)(2,1)} fusion(bf16[320,2048]{1,0:T(8,128)(2,1)S(1)} %bitcast.38, s32[1024]{0:T(1024)S(1)} %pad_clamp_fusion), kind=kCustom, calls=%fused_computation.1 | custom fusion | bytes 2098176 | tf_op jit(solution)/shard_map/gather | solution.py:94
  213.0 2.4 %reshape.85 = f32[128,2,2048]{2,1,0:T(2,128)S(1)} reshape(bf16[256,2048]{1,0:T(8,128)(2,1)} %gather_fusion.1) | data formatting | bytes 3145728 | tf_op jit(solution)/shard_map/convert_element_type | solution.py:94
  215.4 3.9 %multiply_reduce_fusion = bf16[128,2048]{1,0:T(8,128)(2,1)} fusion(f32[128,2,2048]{2,1,0:T(2,128)S(1)} %reshape.85, f32[128,2]{1,0:T(8,128)S(1)} %copy.18), kind=kLoop, calls=%fused_computation.10 | loop fusion | flops 786432 | bytes 2622464 | tf_op jit(solution)/shard_map/reduce_sum | solution.py:95
  219.3 0.0 reduce-scatter.3.cloned.1.call-done
  (13 shorter events, 0.2 us)
Async XLA Ops:
  7.2 172.6 %copy-start = (bf16[256,2048]{1,0:T(8,128)(2,1)S(1)}, bf16[256,2048]{1,0:T(8,128)(2,1)}, u32[]{:S(2)}) copy-start(bf16[256,2048]{1,0:T(8,128)(2,1)} %param.16) | copy-start | bytes 3145732
  7.2 87.7 %all-gather.2.cloned.1.call-start = ((), (), s32[]{:S(2)}) async-start(), calls=%async_computation.5 | async-start | bytes 6553600 | tf_op jit(solution)/shard_map/all_gather | solution.py:80
  55.3 118.7 %reduce-scatter.5.cloned.1.call-start = ((), (), s32[]{:S(2)}) async-start(), calls=%async_computation.6 | async-start | bytes 6553600 | tf_op jit(solution)/shard_map/reduce_scatter | solution.py:85
  122.4 0.9 copy-start.2
  122.4 1.0 copy-start.3
  122.4 57.3 %copy-start.4 = (f32[3,256]{1,0:T(4,128)S(1)}, f32[3,256]{1,0:T(4,128)}, u32[]{:S(2)}) copy-start(f32[3,256]{1,0:T(4,128)} %param.15) | copy-start | bytes 9220
  122.4 57.3 %copy-start.1 = (bf16[256,256]{1,0:T(8,128)(2,1)S(1)}, bf16[256,256]{1,0:T(8,128)(2,1)}, u32[]{:S(2)}) copy-start(bf16[256,256]{1,0:T(8,128)(2,1)} %param.13) | copy-start | bytes 393220
  123.4 57.9 %copy-start.5 = (f32[128,2]{0,1:T(2,128)S(1)}, f32[128,2]{0,1:T(2,128)}, u32[]{:S(2)}) copy-start(f32[128,2]{0,1:T(2,128)} %param.20) | copy-start | bytes 3076
  123.4 56.3 %collective-permute-start = (f32[2,256]{1,0:T(2,128)S(1)}, f32[2,256]{1,0:T(2,128)S(1)}, u32[]{:S(2)}, u32[]{:S(2)}) collective-permute-start(f32[2,256]{1,0:T(2,128)S(1)} %slice.36), channel_id=1, source_target_pairs={{0,4},{4,8},{8,12},{12,16},{16,20},{20,24},{24,28},{1,5},{5,9},{9,... | collective-permute-start | bytes 6152 | tf_op jit(solution)/shard_map/ppermute | solution.py:12
  174.0 36.7 %all-to-all-start.1 = ((bf16[8,40,2048]{2,1,0:T(8,128)(2,1)}), bf16[8,40,2048]{2,1,0:T(8,128)(2,1)S(1)}, u32[]{:S(2)}, u32[]{:S(2)}) async-start(bf16[8,40,2048]{2,1,0:T(8,128)(2,1)} %bitcast.41), calls=%async_computation.3 | async-start | bytes 2621440 | tf_op jit(solution)/shard_map/all_to_all | solution.py:91
  179.5 39.9 %reduce-scatter.3.cloned.1.call-start = ((), (), s32[]{:S(2)}) async-start(), calls=%async_computation.4 | async-start | bytes 1310720 | tf_op jit(solution)/shard_map/reduce_scatter | solution.py:57
Sparse Core Ops, SparseCore 0:
  55.4 39.4 all-gather.1
  122.6 51.3 reduce-scatter.4
  183.4 25.2 reduce-scatter.2
where the time goes:
time: 226 us
  waiting for transfers between devices  116 us (51%)
  blocking collectives  38.6 us (17%)
  matrix products  29 us (13%)
  between operations  13.9 us (6%)
  local copies, waits for them, and re-layouts  11.3 us (5%)
  starting transfers between devices  9.19 us (4%)
  other arithmetic  7.85 us (3%)
    reduce_scatter x1, waiting for transfers between devices, on_device(): lax.psum_scatter(jnp.dot(piece, w_down[0], preferred_element_type=jnp.flo...  47.2 us
    all_gather x1, waiting for transfers between devices, on_device(): piece = lax.all_gather(arrived, 'tp', axis=0, tiled=True)  39.5 us
    all_to_all x1, blocking collectives, on_device(): lax.all_to_all(outgoing, 'ep', split_axis=0, concat_axis=1, tiled=True)  38.6 us
    all_to_all x1, waiting for transfers between devices, on_device(): lax.all_to_all(expert_out.reshape(n_ep, capacity, width), 'ep', split_axi...  29.3 us
    dot_general x1, matrix products, on_device(): jnp.dot(piece, w_down[0], preferred_element_type=jnp.float32)  17.6 us
    dot_general x1, matrix products, on_device(): gate_val = jnp.dot(piece, w_gate[0], preferred_element_type=jnp.float32)  9.98 us
    all_to_all x1, starting transfers between devices, on_device(): lax.all_to_all(expert_out.reshape(n_ep, capacity, width), 'ep', split_axi...  5.52 us
  transfers between devices with their start and end apart: 5, of which 3 were waited for; matrix products, arithmetic and copies ran while one was open for 5% of the time, Pallas kernels for 0%

commit v1 on v0

--- a/solution.py
+++ b/solution.py
@@ -4,6 +4,16 @@
 from jax.sharding import PartitionSpec as P
 
 EPS = 1e-06
+
+
+def turned_line(x, mesh_axis, dim):
+    devices = lax.axis_size(mesh_axis)
+    current, blocks = (x, [x])
+    for _ in range(devices - 1):
+        current = lax.ppermute(current, mesh_axis, [(i, (i + 1) % devices) for i in range(devices)])
+        blocks.insert(0, current)
+    line = jnp.concatenate(blocks, axis=dim)
+    return jnp.roll(line, (lax.axis_index(mesh_axis) + 1) * x.shape[dim], axis=dim)
 
 
 def passed_along(block, axis, distance):
@@ -77,7 +87,7 @@
     arrived = lax.all_to_all(outgoing, "ep", split_axis=0, concat_axis=1, tiled=True).reshape(
         -1, width
     )
-    piece = lax.all_gather(arrived, "tp", axis=0, tiled=True)
+    piece = turned_line(arrived, "tp", 0)
     gate_val = jnp.dot(piece, w_gate[0], preferred_element_type=jnp.float32)
     up_val = jnp.dot(piece, w_up[0], preferred_element_type=jnp.float32)
     hidden = (jax.nn.silu(gate_val) * up_val).astype(jnp.bfloat16)

time: 226 us -> 238 us (1.053)
  waiting for transfers between devices: 116 us -> 127 us
  local copies, waits for them, and re-layouts: 11.3 us -> 20 us
  matrix products: 29 us -> 20.5 us
    ppermute x0 -> x3, waiting for transfers between devices: none -> 51.5 us  [turned_line(): lax.ppermute(current, mesh_axis, [(i, (i + 1) % devices) for i in range(d...]
    all_gather x1 -> x0, waiting for transfers between devices: 39.5 us -> none  [on_device(): piece = lax.all_gather(arrived, 'tp', axis=0, tiled=True)]
    dot_general x1, matrix products: 17.6 us -> 7.4 us  [on_device(): jnp.dot(piece, w_down[0], preferred_element_type=jnp.float32)]
    unnamed x14 -> x31, local copies, waits for them, and re-layouts: 1.92 us -> 9.93 us
    dot_general x0 -> x1, matrix products: none -> 5.96 us  [on_device(): up_val = jnp.dot(piece, w_up[0], preferred_element_type=jnp.float32)]
    dot_general x1, matrix products: 9.98 us -> 5.63 us  [on_device(): gate_val = jnp.dot(piece, w_gate[0], preferred_element_type=jnp.float32)]
  transfers between devices with their start and end apart: 5 -> 7, of which waited for: 3 -> 5; matrix products, arithmetic and copies ran while one was open for 5% -> 4% of each run, Pallas kernels for 0% -> 0%
where the time goes in v1:
time: 238 us; the launch traced here: 237 us
  waiting for transfers between devices  127 us (53%)
  blocking collectives  38.7 us (16%)
  matrix products  20.5 us (9%)
  local copies, waits for them, and re-layouts  20 us (8%)
  between operations  14.3 us (6%)
  starting transfers between devices  9.13 us (4%)
  other arithmetic  7.85 us (3%)
    ppermute x3, waiting for transfers between devices, turned_line(): lax.ppermute(current, mesh_axis, [(i, (i + 1) % devices) for i in range(d...  51.5 us
    reduce_scatter x1, waiting for transfers between devices, on_device(): lax.psum_scatter(jnp.dot(piece, w_down[0], preferred_element_type=jnp.flo...  46.2 us
    all_to_all x1, blocking collectives, on_device(): lax.all_to_all(outgoing, 'ep', split_axis=0, concat_axis=1, tiled=True)  38.7 us
    all_to_all x1, waiting for transfers between devices, on_device(): lax.all_to_all(expert_out.reshape(n_ep, capacity, width), 'ep', split_axi...  29.3 us
    unnamed x31, local copies, waits for them, and re-layouts  9.93 us
    dot_general x1, matrix products, on_device(): jnp.dot(piece, w_down[0], preferred_element_type=jnp.float32)  7.4 us
    dot_general x1, matrix products, on_device(): up_val = jnp.dot(piece, w_up[0], preferred_element_type=jnp.float32)  5.96 us
    dot_general x1, matrix products, on_device(): gate_val = jnp.dot(piece, w_gate[0], preferred_element_type=jnp.float32)  5.63 us
  transfers between devices with their start and end apart: 7, of which 5 were waited for; matrix products, arithmetic and copies ran while one was open for 4% of the time, Pallas kernels for 0%

profile of v1, /device:TPU:0, one launch (start us, length us, event | category | flops | bytes accessed | tf_op | source)
XLA Modules:
  0.0 237.5 jit_solution(3511571550131706064)
XLA Ops:
  7.2 0.0 copy-start
  7.2 0.0 reduce-scatter.5.cloned.1.call-start
  7.2 0.9 copy.16
  8.1 0.1 eq.32
  8.2 0.1 eq.28
  8.4 0.7 broadcast_multiply_fusion
  9.1 0.6 reduce-window.6
  9.6 0.2 slice_reduce_fusion
  9.9 0.1 copy.15
  10.0 0.1 mul.110
  10.1 0.1 fusion.26
  10.3 1.4 scatter_custom_fusion
  11.7 1.2 fusion.11
  12.9 1.2 fusion.13
  14.2 3.0 %gather_fusion = bf16[320,2048]{1,0:T(8,128)(2,1)} fusion(bf16[129,2048]{1,0:T(8,128)(2,1)S(1)} %concatenate.13, s32[1024]{0:T(1024)S(1)} %pad_clamp_fusion.1), kind=kCustom, calls=%fused_computation | custom fusion | bytes 2622720 | tf_op jit(solution)/shard_map/gather | solution.py:40
  17.3 38.7 %all_to_all.14 = bf16[8,40,2048]{2,1,0:T(8,128)(2,1)S(1)} all-to-all(bf16[8,40,2048]{2,1,0:T(8,128)(2,1)} %bitcast.34), channel_id=1, replica_groups=mesh['ep'=8,'tp'=4] {'ep'}, dimensions={0} | all-to-all | bytes 2621440 | tf_op jit(solution)/shard_map/all_to_all | solution.py:87
  56.0 17.0 %collective-permute-done.1 = bf16[320,2048]{1,0:T(8,128)(2,1)S(1)} collective-permute-done((bf16[320,2048]{1,0:T(8,128)(2,1)S(1)}, bf16[320,2048]{1,0:T(8,128)(2,1)S(1)}, u32[]{:S(2)}, u32[]{:S(2)}) %collective-permute-start.1) | collective-permute-done | bytes 1310752 | tf_op jit(solution)/shard_map/ppermute | solution.py:13
  73.0 1.1 copy-done.1
  74.1 17.1 %collective-permute-done.2 = bf16[320,2048]{1,0:T(8,128)(2,1)} collective-permute-done((bf16[320,2048]{1,0:T(8,128)(2,1)S(1)}, bf16[320,2048]{1,0:T(8,128)(2,1)}, u32[]{:S(2)}, u32[]{:S(2)}) %collective-permute-start.2) | collective-permute-done | bytes 1310752 | tf_op jit(solution)/shard_map/ppermute | solution.py:13
  91.2 17.3 %collective-permute-done.3 = bf16[320,2048]{1,0:T(8,128)(2,1)} collective-permute-done((bf16[320,2048]{1,0:T(8,128)(2,1)}, bf16[320,2048]{1,0:T(8,128)(2,1)}, u32[]{:S(2)}, u32[]{:S(2)}) %collective-permute-start.3) | collective-permute-done | bytes 1310752 | tf_op jit(solution)/shard_map/ppermute | solution.py:13
  108.6 1.4 constant_dynamic-update-slice_fusion.7
  110.0 1.5 constant_dynamic-update-slice_fusion.6
  111.5 0.1 constant_dynamic-update-slice_fusion.5
  111.6 0.1 constant_dynamic-update-slice_fusion.4
  111.7 1.5 constant_dynamic-update-slice_fusion.3
  113.2 0.0 copy-start.8
  113.2 1.6 constant_dynamic-update-slice_fusion.2
  114.8 0.1 constant_dynamic-update-slice_fusion.1
  115.0 0.1 constant_dynamic-update-slice_fusion
  115.1 0.6 copy-done.8
  115.6 5.6 %fusion.2 = f32[1280,896]{1,0:T(8,128)S(1)} fusion(bf16[2560,2048]{1,0:T(8,128)(2,1)S(1)} %constant_dynamic-update-slice_fusion, s32[]{:T(128)S(6)} %select_n.36, bf16[1,2048,896]{2,1,0:T(8,128)(2,1)S(1)} %copy-done.8), kind=kOutput, calls=%fused_computation.6 | convolution fusion | flops 4697620480 | bytes 13500420 | tf_op jit(solution)/shard_map/dot_general | solution.py:91
  121.3 0.0 copy-start.10
  121.3 6.0 %multiply_convert_fusion = bf16[1280,896]{1,0:T(8,128)(2,1)S(1)} fusion(f32[1280,896]{1,0:T(8,128)S(1)} %fusion.2, bf16[1,2048,896]{2,1,0:T(8,128)(2,1)S(1)} %copy-done.9, bf16[2560,2048]{1,0:T(8,128)(2,1)S(1)} %constant_dynamic-update-slice_fusion, s32[]{:T(128)S(6)} %select_n.36), kind=kOutput, calls=%fused_computation.8 | convolution fusion | flops 4704501760 | bytes 15794180 | tf_op jit(solution)/shard_map/dot_general | solution.py:92
  127.3 7.4 %convolution_convert_fusion = bf16[1280,2048]{1,0:T(8,128)(2,1)} fusion(bf16[1280,896]{1,0:T(8,128)(2,1)S(1)} %multiply_convert_fusion, bf16[1,896,2048]{2,1,0:T(8,128)(2,1)S(1)} %copy-done.10), kind=kOutput, calls=%fused_computation.3 | convolution fusion | flops 4700241920 | bytes 11206656 | tf_op jit(solution)/shard_map/dot_general | solution.py:96
  134.7 0.0 reduce-scatter.5.cloned.1.call-update
  134.7 0.9 copy-done.4
  135.6 0.1 copy-done.5
  135.7 3.3 %collective-permute-start = (f32[2,256]{1,0:T(2,128)S(1)}, f32[2,256]{1,0:T(2,128)S(1)}, u32[]{:S(2)}, u32[]{:S(2)}) collective-permute-start(f32[2,256]{1,0:T(2,128)S(1)} %slice.36), channel_id=1, source_target_pairs={{0,4},{4,8},{8,12},{12,16},{16,20},{20,24},{24,28},{1,5},{5,9},{9,... | collective-permute-start | bytes 6152 | tf_op jit(solution)/shard_map/ppermute | solution.py:22
  139.0 46.2 %reduce-scatter.5.cloned.1.call-done = bf16[320,2048]{1,0:T(8,128)(2,1)} async-done(((bf16[1280,2048]{1,0:T(8,128)(2,1)}), bf16[320,2048]{1,0:T(8,128)(2,1)}) %reduce-scatter.5.cloned.1.call-update) | async-done | bytes 1310736 | tf_op jit(solution)/shard_map/reduce_scatter | solution.py:95
  185.2 5.5 %all-to-all-start.1 = ((bf16[8,40,2048]{2,1,0:T(8,128)(2,1)}), bf16[8,40,2048]{2,1,0:T(8,128)(2,1)S(1)}, u32[]{:S(2)}, u32[]{:S(2)}) async-start(bf16[8,40,2048]{2,1,0:T(8,128)(2,1)} %bitcast.35), calls=%async_computation.3 | async-start | bytes 2621440 | tf_op jit(solution)/shard_map/all_to_all | solution.py:101
  190.7 0.3 reduce-scatter.3.cloned.1.call-start
  191.0 1.5 convolution_convert_fusion.1
  192.5 0.0 reduce-scatter.3.cloned.1.call-update
  192.5 0.1 copy.18
  192.7 29.3 %all-to-all-done.1 = bf16[8,40,2048]{2,1,0:T(8,128)(2,1)S(1)} async-done(((bf16[8,40,2048]{2,1,0:T(8,128)(2,1)}), bf16[8,40,2048]{2,1,0:T(8,128)(2,1)S(1)}, u32[]{:S(2)}, u32[]{:S(2)}) %all-to-all-start.1) | async-done | bytes 1310752 | tf_op jit(solution)/shard_map/all_to_all | solution.py:101
  221.9 2.4 %gather_fusion.1 = bf16[256,2048]{1,0:T(8,128)(2,1)} fusion(bf16[320,2048]{1,0:T(8,128)(2,1)S(1)} %bitcast.30, s32[1024]{0:T(1024)S(1)} %pad_clamp_fusion), kind=kCustom, calls=%fused_computation.1 | custom fusion | bytes 2098176 | tf_op jit(solution)/shard_map/gather | solution.py:104
  224.3 2.4 reshape.85
  226.7 3.9 %multiply_reduce_fusion = bf16[128,2048]{1,0:T(8,128)(2,1)} fusion(f32[128,2,2048]{2,1,0:T(2,128)S(1)} %reshape.85, f32[128,2]{1,0:T(8,128)S(1)} %copy.18), kind=kLoop, calls=%fused_computation.13 | loop fusion | flops 786432 | bytes 2622464 | tf_op jit(solution)/shard_map/reduce_sum | solution.py:105
  (33 shorter events, 0.2 us)
Async XLA Ops:
  7.2 183.9 %copy-start = (bf16[256,2048]{1,0:T(8,128)(2,1)S(1)}, bf16[256,2048]{1,0:T(8,128)(2,1)}, u32[]{:S(2)}) copy-start(bf16[256,2048]{1,0:T(8,128)(2,1)} %param.16) | copy-start | bytes 3145732
  7.2 178.0 %reduce-scatter.5.cloned.1.call-start = ((), (), s32[]{:S(2)}) async-start(), calls=%async_computation.5 | async-start | bytes 6553600 | tf_op jit(solution)/shard_map/reduce_scatter | solution.py:95
  55.9 17.0 %collective-permute-start.1 = (bf16[320,2048]{1,0:T(8,128)(2,1)S(1)}, bf16[320,2048]{1,0:T(8,128)(2,1)S(1)}, u32[]{:S(2)}, u32[]{:S(2)}) collective-permute-start(bf16[320,2048]{1,0:T(8,128)(2,1)S(1)} %bitcast.31), channel_id=1, source_target_pairs={{0,1},{1,2},{2,3},{3,0},{4,5},{5,6},{6,7},{7,4},{8,9},{9,10},{10,1... | collective-permute-start | bytes 3932168 | tf_op jit(solution)/shard_map/ppermute | solution.py:13
  73.0 1.1 copy-start.1
  74.1 17.1 %collective-permute-start.2 = (bf16[320,2048]{1,0:T(8,128)(2,1)S(1)}, bf16[320,2048]{1,0:T(8,128)(2,1)}, u32[]{:S(2)}, u32[]{:S(2)}) collective-permute-start(bf16[320,2048]{1,0:T(8,128)(2,1)S(1)} %collective-permute-done.1), channel_id=1, source_target_pairs={{0,1},{1,2},{2,3},{3,0},{4,5},{5,6},{6,7},{7,4},{8,9},{9,10},{10,1... | collective-permute-start | bytes 3932168 | tf_op jit(solution)/shard_map/ppermute | solution.py:13
  91.2 17.3 %collective-permute-start.3 = (bf16[320,2048]{1,0:T(8,128)(2,1)}, bf16[320,2048]{1,0:T(8,128)(2,1)}, u32[]{:S(2)}, u32[]{:S(2)}) collective-permute-start(bf16[320,2048]{1,0:T(8,128)(2,1)} %collective-permute-done.2), channel_id=1, source_target_pairs={{0,1},{1,2},{2,3},{3,0},{4,5},{5,6},{6,7},{7,4},{8,9},{9,10},{10,1... | collective-permute-start | bytes 3932168 | tf_op jit(solution)/shard_map/ppermute | solution.py:13
  91.2 20.3 %copy-start.2 = (bf16[320,2048]{1,0:T(8,128)(2,1)S(1)}, bf16[320,2048]{1,0:T(8,128)(2,1)}, u32[]{:S(2)}) copy-start(bf16[320,2048]{1,0:T(8,128)(2,1)} %copy-done.1) | copy-start | bytes 3932164
  113.2 2.4 %copy-start.8 = (bf16[1,2048,896]{2,1,0:T(8,128)(2,1)S(1)}, bf16[1,2048,896]{2,1,0:T(8,128)(2,1)}, u32[]{:S(2)}) copy-start(bf16[1,2048,896]{2,1,0:T(8,128)(2,1)} %param.21) | copy-start | bytes 11010052
  115.6 5.6 %copy-start.9 = (bf16[1,2048,896]{2,1,0:T(8,128)(2,1)S(1)}, bf16[1,2048,896]{2,1,0:T(8,128)(2,1)}, u32[]{:S(2)}) copy-start(bf16[1,2048,896]{2,1,0:T(8,128)(2,1)} %param.22) | copy-start | bytes 11010052
  121.3 6.0 %copy-start.10 = (bf16[1,896,2048]{2,1,0:T(8,128)(2,1)S(1)}, bf16[1,896,2048]{2,1,0:T(8,128)(2,1)}, u32[]{:S(2)}) copy-start(bf16[1,896,2048]{2,1,0:T(8,128)(2,1)} %param.23) | copy-start | bytes 11010052
  134.7 0.9 copy-start.4
  134.7 1.0 copy-start.5
  134.7 56.3 %copy-start.6 = (f32[3,256]{1,0:T(4,128)S(1)}, f32[3,256]{1,0:T(4,128)}, u32[]{:S(2)}) copy-start(f32[3,256]{1,0:T(4,128)} %param.15) | copy-start | bytes 9220
  134.7 56.4 %copy-start.3 = (bf16[256,256]{1,0:T(8,128)(2,1)S(1)}, bf16[256,256]{1,0:T(8,128)(2,1)}, u32[]{:S(2)}) copy-start(bf16[256,256]{1,0:T(8,128)(2,1)} %param.13) | copy-start | bytes 393220
  135.6 56.9 %copy-start.7 = (f32[128,2]{0,1:T(2,128)S(1)}, f32[128,2]{0,1:T(2,128)}, u32[]{:S(2)}) copy-start(f32[128,2]{0,1:T(2,128)} %param.20) | copy-start | bytes 3076
  135.7 55.3 %collective-permute-start = (f32[2,256]{1,0:T(2,128)S(1)}, f32[2,256]{1,0:T(2,128)S(1)}, u32[]{:S(2)}, u32[]{:S(2)}) collective-permute-start(f32[2,256]{1,0:T(2,128)S(1)} %slice.36), channel_id=1, source_target_pairs={{0,4},{4,8},{8,12},{12,16},{16,20},{20,24},{24,28},{1,5},{5,9},{9,... | collective-permute-start | bytes 6152 | tf_op jit(solution)/shard_map/ppermute | solution.py:22
  185.2 36.7 %all-to-all-start.1 = ((bf16[8,40,2048]{2,1,0:T(8,128)(2,1)}), bf16[8,40,2048]{2,1,0:T(8,128)(2,1)S(1)}, u32[]{:S(2)}, u32[]{:S(2)}) async-start(bf16[8,40,2048]{2,1,0:T(8,128)(2,1)} %bitcast.35), calls=%async_computation.3 | async-start | bytes 2621440 | tf_op jit(solution)/shard_map/all_to_all | solution.py:101
  190.7 39.9 %reduce-scatter.3.cloned.1.call-start = ((), (), s32[]{:S(2)}) async-start(), calls=%async_computation.4 | async-start | bytes 1310720 | tf_op jit(solution)/shard_map/reduce_scatter | solution.py:67
Sparse Core Ops, SparseCore 0:
  134.8 50.3 reduce-scatter.4
  194.6 25.2 reduce-scatter.2
